TPU v7x, 32 devices: a whole 2x2x4 slice. The times are simulated.
32 devices in a mesh: kv: 4 (over y, x), tp: 8 (over z, core).
Axes of the slice: x: 2, y: 2, z: 4, core: 2. Of those that a mesh axis runs over, the one named last changes fastest.
Arguments:
- tokens: bfloat16 [64, 4096], P('tp', 'kv'), may hold values from -100 to 100
- state: float32 [64, 32, 128, 128], P('kv', 'tp'), may hold values from -3 to 3
- gain_pre: bfloat16 [4096], P('kv'), may hold values from 0.099609375 to 1.8984375
- w_gate_pre: bfloat16 [4096, 11264], P('kv', 'tp'), may hold values from -0.09375 to 0.09375
- w_up_pre: bfloat16 [4096, 11264], P('kv', 'tp'), may hold values from -0.09375 to 0.09375
- w_down_pre: bfloat16 [11264, 4096], P('tp', 'kv'), may hold values from -0.109375 to 0.109375
- gain_mix: bfloat16 [4096], P('kv'), may hold values from 0.099609375 to 1.8984375
- w_query: bfloat16 [4096, 4096], P('kv', 'tp'), may hold values from -0.09375 to 0.09375
- w_key: bfloat16 [4096, 4096], P('kv', 'tp'), may hold values from -0.09375 to 0.09375
- w_value: bfloat16 [4096, 4096], P('kv', 'tp'), may hold values from -0.09375 to 0.09375
- w_decay: bfloat16 [4096, 32], P('kv'), may hold values from -0.09375 to 0.09375
- w_blend: bfloat16 [4096, 32], P('kv'), may hold values from -0.09375 to 0.09375
- decay_base: float32 [32], P('tp'), may hold values from -3 to 0.7
- decay_shift: float32 [32], P('tp'), may hold values from -2 to 0.5
- head_gain: bfloat16 [128], replicated, may hold values from 0.099609375 to 1.8984375
- w_out: bfloat16 [4096, 4096], P('tp', 'kv'), may hold values from -0.09375 to 0.09375
- gain_post: bfloat16 [4096], P('kv'), may hold values from 0.099609375 to 1.8984375
- w_gate_post: bfloat16 [4096, 11264], P('kv', 'tp'), may hold values from -0.09375 to 0.09375
- w_up_post: bfloat16 [4096, 11264], P('kv', 'tp'), may hold values from -0.09375 to 0.09375
- w_down_post: bfloat16 [11264, 4096], P('tp', 'kv'), may hold values from -0.109375 to 0.109375
Outputs:
- result: bfloat16 [64, 4096], P('tp', 'kv')
- new_state: float32 [64, 32, 128, 128], P('kv', 'tp')
All inputs are finite; a program needn't handle non-finite values.
Results may differ from a plain program's by a relative error of at most 0.015.
Values may be sent and summed in bfloat16 or wider, within the bound.
A program may use at most 64 MiB of HBM per device.

v0:
```python
import jax
import jax.numpy as jnp
from jax import lax
from jax.sharding import PartitionSpec as P

D = 4096


EPS = 1e-06


def spread(own_rows):
    return lax.all_gather(own_rows, "tp", axis=0, tiled=True)


def inverse_rms(stream):
    values = stream.astype(jnp.float32)
    squares = lax.psum(jnp.sum(values * values, axis=1), "kv")
    return lax.rsqrt(squares / D + EPS)[:, None]


def gained(stream, gain_vec):
    return (stream.astype(jnp.float32) * gain_vec.astype(jnp.float32)).astype(jnp.bfloat16)


def residual_add(stream, branch, weight):
    return (stream.astype(jnp.float32) + weight * branch).astype(jnp.bfloat16)


def unit_rows(values):
    return values * lax.rsqrt(jnp.sum(values * values, axis=-1, keepdims=True) + EPS)


def kv_rows(values):
    count = values.shape[0] // lax.axis_size("kv")
    return lax.dynamic_slice_in_dim(values, lax.axis_index("kv") * count, count, 0)


def half_block(stream, gain_vec, w_gate, w_up, w_down):
    factor = inverse_rms(stream)
    scaled = gained(stream, gain_vec)
    gate_part = jnp.dot(scaled, w_gate, preferred_element_type=jnp.float32)
    up_part = jnp.dot(scaled, w_up, preferred_element_type=jnp.float32)
    gate_sum, up_sum = (
        lax.psum(gate_part.astype(jnp.bfloat16), "kv").astype(jnp.float32),
        lax.psum(up_part.astype(jnp.bfloat16), "kv").astype(jnp.float32),
    )
    hidden = (jax.nn.silu(factor * gate_sum) * (factor * up_sum)).astype(jnp.bfloat16)
    return jnp.dot(hidden, w_down, preferred_element_type=jnp.float32)


def settle(partial_value):
    return lax.psum_scatter(
        partial_value.astype(jnp.bfloat16), "tp", scatter_dimension=0, tiled=True
    ).astype(jnp.float32)


def advance(own_rows, partial_value, weight):
    own_rows = residual_add(own_rows, settle(partial_value), weight)
    return (spread(own_rows), own_rows)


def on_device(
    tokens,
    state,
    gain_pre,
    w_gate_pre,
    w_up_pre,
    w_down_pre,
    gain_mix,
    w_query,
    w_key,
    w_value,
    w_decay,
    w_blend,
    decay_base,
    decay_shift,
    head_gain,
    w_out,
    gain_post,
    w_gate_post,
    w_up_post,
    w_down_post,
):
    own_rows = tokens
    stream = spread(own_rows)
    partial_value = half_block(stream, gain_pre, w_gate_pre, w_up_pre, w_down_pre)
    stream, own_rows = advance(own_rows, partial_value, 0.5)
    factor = inverse_rms(stream)
    scaled = gained(stream, gain_mix)
    queries, keys_new, values_new, decay_in, blend_in = (
        lax.psum_scatter(
            jnp.dot(scaled, w_query, preferred_element_type=jnp.float32).astype(jnp.bfloat16),
            "kv",
            scatter_dimension=0,
            tiled=True,
        ).astype(jnp.float32),
        lax.psum_scatter(
            jnp.dot(scaled, w_key, preferred_element_type=jnp.float32).astype(jnp.bfloat16),
            "kv",
            scatter_dimension=0,
            tiled=True,
        ).astype(jnp.float32),
        lax.psum_scatter(
            jnp.dot(scaled, w_value, preferred_element_type=jnp.float32).astype(jnp.bfloat16),
            "kv",
            scatter_dimension=0,
            tiled=True,
        ).astype(jnp.float32),
        lax.psum_scatter(
            jnp.dot(scaled, w_decay, preferred_element_type=jnp.float32).astype(jnp.bfloat16),
            "kv",
            scatter_dimension=0,
            tiled=True,
        ).astype(jnp.float32),
        lax.psum_scatter(
            jnp.dot(scaled, w_blend, preferred_element_type=jnp.float32).astype(jnp.bfloat16),
            "kv",
            scatter_dimension=0,
            tiled=True,
        ).astype(jnp.float32),
    )
    own_factor = kv_rows(factor)
    seqs = state.shape[0]
    heads_dev = state.shape[1]
    head_dim = state.shape[3]
    queries = unit_rows((own_factor * queries).reshape(seqs, heads_dev, head_dim)) * head_dim ** (
        -0.5
    )
    keys_unit = unit_rows((own_factor * keys_new).reshape(seqs, heads_dev, head_dim))
    values_new = (own_factor * values_new).reshape(seqs, heads_dev, head_dim)
    head_start = lax.axis_index("tp") * heads_dev
    decay_in = lax.dynamic_slice_in_dim(own_factor * decay_in, head_start, heads_dev, 1)
    blend_in = lax.dynamic_slice_in_dim(own_factor * blend_in, head_start, heads_dev, 1)
    log_rate = -jnp.exp(decay_base) * jax.nn.softplus(decay_in + decay_shift)
    rate = jnp.exp(log_rate)
    beta = jax.nn.sigmoid(blend_in)
    recalled = jnp.einsum("bhk,bhkv->bhv", keys_unit, state, precision=lax.Precision.HIGHEST)
    correction = beta[:, :, None] * (values_new - rate[:, :, None] * recalled)
    new_state = (
        rate[:, :, None, None] * state + keys_unit[:, :, :, None] * correction[:, :, None, :]
    )
    read_out = jnp.einsum("bhk,bhkv->bhv", queries, new_state, precision=lax.Precision.HIGHEST)
    normed = read_out * lax.rsqrt(jnp.mean(read_out * read_out, axis=2, keepdims=True) + EPS)
    normed = (
        (normed * head_gain.astype(jnp.float32))
        .astype(jnp.bfloat16)
        .reshape(seqs, heads_dev * head_dim)
    )
    partial_value = jnp.dot(
        lax.all_gather(normed, "kv", axis=0, tiled=True), w_out, preferred_element_type=jnp.float32
    )
    stream, own_rows = advance(own_rows, partial_value, 1.0)
    partial_value = half_block(stream, gain_post, w_gate_post, w_up_post, w_down_post)
    result = residual_add(own_rows, settle(partial_value), 0.5)
    return (result, new_state)


def solution(mesh):
    return jax.shard_map(
        on_device,
        mesh=mesh,
        in_specs=(
            P("tp", "kv"),
            P("kv", "tp", None, None),
            P("kv"),
            P("kv", "tp"),
            P("kv", "tp"),
            P("tp", "kv"),
            P("kv"),
            P("kv", "tp"),
            P("kv", "tp"),
            P("kv", "tp"),
            P("kv", None),
            P("kv", None),
            P("tp"),
            P("tp"),
            P(),
            P("tp", "kv"),
            P("kv"),
            P("kv", "tp"),
            P("kv", "tp"),
            P("tp", "kv"),
        ),
        out_specs=(P("tp", "kv"), P("kv", "tp", None, None)),
        check_vma=False,
    )
```

profile of v0, /device:TPU:0, one launch (start us, length us, event | category | flops | bytes accessed | tf_op | source)
XLA Modules:
  0.0 365.2 jit_solution(18291495308764507529)
XLA Ops:
  7.2 0.0 all-reduce.10.cloned.1.call-start
  7.2 0.8 convert_element_type.134
  8.1 16.1 %all_gather.12 = bf16[64,1024]{1,0:T(8,128)(2,1)S(1)} all-gather(bf16[8,1024]{1,0:T(8,128)(2,1)} %param.20), channel_id=1, replica_groups=mesh['kv'=4,'tp'=8] {'tp'}, dimensions={0}, use_global_device_ids=true | all-gather | bytes 147456 | tf_op jit(solution)/shard_map/all_gather | solution.py:13
  24.1 1.3 convolution_convert_fusion.2
  25.4 1.3 convolution_convert_fusion.3
  26.7 0.0 all-reduce.10.cloned.1.call-update
  26.7 0.0 reduce-scatter.7.cloned.1.call-start
  26.8 0.1 fusion
  26.9 10.0 %psum.49 = f32[64]{0:T(128)S(1)} all-reduce(f32[64]{0:T(128)S(1)} %fusion), channel_id=1, replica_groups=mesh['kv'=4,'tp'=8] {'kv'}, use_global_device_ids=true, to_apply=%region_1.0 | all-reduce | flops 64 | bytes 512 | tf_op jit(solution)/shard_map/psum | solution.py:18
  36.9 34.9 %all-reduce.10.cloned.1.call-done = (bf16[64,1408]{1,0:T(8,128)(2,1)}, bf16[64,1408]{1,0:T(8,128)(2,1)}) async-done(((bf16[64,1408]{1,0:T(8,128)(2,1)}, bf16[64,1408]{1,0:T(8,128)(2,1)}), (bf16[64,1408]{1,0:T(8,128)(2,1)}, bf16[64,1408]{1,0:T(8,128)(2,1)})) %all-reduce.10.cloned.1.call-update) | async-done | bytes 360464 | tf_op jit(solution)/shard_map/psum | solution.py:46
  71.8 3.4 convolution_convert_fusion.6
  75.2 0.0 reduce-scatter.11.cloned.1.call-start
  75.3 0.6 dynamic-slice.1
  76.6 29.4 %reduce-scatter.7.cloned.1.call-done = bf16[8,1024]{1,0:T(8,128)(2,1)} async-done(((bf16[64,1024]{1,0:T(8,128)(2,1)}), bf16[8,1024]{1,0:T(8,128)(2,1)}) %reduce-scatter.7.cloned.1.call-update) | async-done | bytes 16400 | tf_op jit(solution)/shard_map/reduce_scatter | solution.py:53
  106.0 0.7 add_convert_fusion.2
  106.7 13.9 %all_gather.13 = bf16[64,1024]{1,0:T(8,128)(2,1)S(1)} all-gather(bf16[8,1024]{1,0:T(8,128)(2,1)S(1)} %add_convert_fusion.2), channel_id=1, replica_groups=mesh['kv'=4,'tp'=8] {'tp'}, dimensions={0}, use_global_device_ids=true | all-gather | bytes 147456 | tf_op jit(solution)/shard_map/all_gather | solution.py:13
  120.6 0.1 fusion.2
  120.8 9.8 %psum.52 = f32[64]{0:T(128)S(1)} all-reduce(f32[64]{0:T(128)S(1)} %fusion.2), channel_id=1, replica_groups=mesh['kv'=4,'tp'=8] {'kv'}, use_global_device_ids=true, to_apply=%region_6.7 | all-reduce | flops 64 | bytes 512 | tf_op jit(solution)/shard_map/psum | solution.py:18
  130.6 0.2 convolution_convert_fusion.11
  130.8 0.2 convolution_convert_fusion.10
  130.9 2.1 convolution_convert_fusion.8
  133.1 0.0 reduce-scatter.11.cloned.1.call-update
  133.1 0.0 reduce-scatter.9.cloned.1.call-start
  133.2 0.1 mul.229
  133.2 14.4 %all-reduce.2 = (bf16[64,32]{1,0:T(8,128)(2,1)S(1)}, bf16[64,32]{1,0:T(8,128)(2,1)S(1)}) all-reduce(bf16[64,32]{1,0:T(8,128)(2,1)S(1)} %convolution_convert_fusion.11, bf16[64,32]{1,0:T(8,128)(2,1)S(1)} %convolution_convert_fusion.10), channel_id=4, replica_groups=mesh['kv'=4,'tp'=8] {'kv'}, use_global_device_ids=true, to_apply=%region_9.10.clone | all-reduce | flops 4096 | bytes 16384
  147.7 2.1 convolution_convert_fusion.9
  149.8 0.0 reduce-scatter.9.cloned.1.call-update
  149.8 0.0 reduce-scatter.13.cloned.1.call-start
  149.9 2.1 convolution_convert_fusion.7
  152.0 0.0 reduce-scatter.13.cloned.1.call-update
  152.0 0.0 reduce-scatter.15.cloned.1.call-start
  152.1 0.1 add_divide_fusion
  152.2 1.6 reduce-scatter.11.cloned.1.call-done
  153.8 26.6 %reduce-scatter.9.cloned.1.call-done = bf16[16,512]{1,0:T(8,128)(2,1)} async-done(((bf16[64,512]{1,0:T(8,128)(2,1)}), bf16[16,512]{1,0:T(8,128)(2,1)}) %reduce-scatter.9.cloned.1.call-update) | async-done | bytes 16400 | tf_op jit(solution)/shard_map/reduce_scatter | solution.py:92
  180.4 26.7 %reduce-scatter.13.cloned.1.call-done = bf16[16,512]{1,0:T(8,128)(2,1)} async-done(((bf16[64,512]{1,0:T(8,128)(2,1)}), bf16[16,512]{1,0:T(8,128)(2,1)}) %reduce-scatter.13.cloned.1.call-update) | async-done | bytes 16400 | tf_op jit(solution)/shard_map/reduce_scatter | solution.py:104
  207.1 0.8 convert_multiply_fusion.7
  207.9 0.1 multiply_reduce_fusion.1
  208.1 0.1 broadcast_multiply_fusion
  208.2 0.1 multiply_reduce_fusion.2
  208.3 0.1 multiply_multiply_fusion
  208.4 5.5 %fusion.23 = f32[16,4,1,128]{3,2,1,0:T(1,128)S(1)} fusion(f32[16,4,128,1]{2,3,1,0:T(1,128)S(1)} %bitcast.32, f32[16,4,128,128]{3,2,1,0:T(8,128)} %param.21), kind=kOutput, calls=%fused_computation.58 | convolution fusion | flops 12582912 | bytes 4259840 | tf_op jit(solution)/shard_map/bhk,bhkv->bhv/dot_general | solution.py:138
  213.9 0.1 subtract_multiply_fusion
  214.0 1.5 multiply_add_fusion
  215.5 2.0 copy-done.2
  217.5 3.7 %fusion.24 = f32[16,4,1,128]{3,2,1,0:T(1,128)S(1)} fusion(f32[16,4,128,1]{2,3,1,0:T(1,128)S(1)} %bitcast.36, f32[16,4,128,128]{3,2,1,0:T(8,128)S(1)} %multiply_add_fusion), kind=kOutput, calls=%fused_computation.59 | convolution fusion | flops 12582912 | bytes 4259840 | tf_op jit(solution)/shard_map/bhk,bhkv->bhv/dot_general | solution.py:143
  221.2 0.1 multiply_reduce_fusion
  221.3 0.1 multiply_convert_fusion.4
  221.4 8.2 %all_gather.14 = bf16[64,512]{1,0:T(8,128)(2,1)S(1)} all-gather(bf16[16,512]{1,0:T(8,128)(2,1)S(1)} %bitcast.38), channel_id=1, replica_groups=mesh['kv'=4,'tp'=8] {'kv'}, dimensions={0}, use_global_device_ids=true | all-gather | bytes 81920 | tf_op jit(solution)/shard_map/all_gather | solution.py:151
  229.6 0.9 convolution_convert_fusion.5
  230.5 0.0 reduce-scatter.15.cloned.1.call-update
  230.5 0.0 all-reduce.8.cloned.1.call-start
  230.6 30.7 %reduce-scatter.15.cloned.1.call-done = bf16[8,1024]{1,0:T(8,128)(2,1)} async-done(((bf16[64,1024]{1,0:T(8,128)(2,1)}), bf16[8,1024]{1,0:T(8,128)(2,1)}) %reduce-scatter.15.cloned.1.call-update) | async-done | bytes 16400 | tf_op jit(solution)/shard_map/reduce_scatter | solution.py:53
  261.3 0.9 add_convert_fusion.1
  262.2 14.1 %all_gather.15 = bf16[64,1024]{1,0:T(8,128)(2,1)S(1)} all-gather(bf16[8,1024]{1,0:T(8,128)(2,1)S(1)} %add_convert_fusion.1), channel_id=1, replica_groups=mesh['kv'=4,'tp'=8] {'tp'}, dimensions={0}, use_global_device_ids=true | all-gather | bytes 147456 | tf_op jit(solution)/shard_map/all_gather | solution.py:13
  276.2 3.1 convolution_convert_fusion
  279.3 1.3 convolution_convert_fusion.1
  280.6 0.0 all-reduce.8.cloned.1.call-update
  280.6 0.0 reduce-scatter.17.cloned.1.call-start
  280.7 0.1 fusion.4
  280.8 10.1 %psum.53 = f32[64]{0:T(128)S(1)} all-reduce(f32[64]{0:T(128)S(1)} %fusion.4), channel_id=1, replica_groups=mesh['kv'=4,'tp'=8] {'kv'}, use_global_device_ids=true, to_apply=%region_17.18 | all-reduce | flops 64 | bytes 512 | tf_op jit(solution)/shard_map/psum | solution.py:18
  290.9 32.0 %all-reduce.8.cloned.1.call-done = (bf16[64,1408]{1,0:T(8,128)(2,1)}, bf16[64,1408]{1,0:T(8,128)(2,1)}) async-done(((bf16[64,1408]{1,0:T(8,128)(2,1)}, bf16[64,1408]{1,0:T(8,128)(2,1)}), (bf16[64,1408]{1,0:T(8,128)(2,1)}, bf16[64,1408]{1,0:T(8,128)(2,1)})) %all-reduce.8.cloned.1.call-update) | async-done | bytes 360464 | tf_op jit(solution)/shard_map/psum | solution.py:46
  322.9 3.3 convolution_convert_fusion.4
  326.3 30.7 %reduce-scatter.17.cloned.1.call-done = bf16[8,1024]{1,0:T(8,128)(2,1)} async-done(((bf16[64,1024]{1,0:T(8,128)(2,1)}), bf16[8,1024]{1,0:T(8,128)(2,1)}) %reduce-scatter.17.cloned.1.call-update) | async-done | bytes 16400 | tf_op jit(solution)/shard_map/reduce_scatter | solution.py:53
  357.0 1.3 add_convert_fusion
  (45 shorter events, 0.2 us)
Async XLA Ops:
  7.2 17.0 %copy-start = (bf16[1024,1408]{1,0:T(8,128)(2,1)S(1)}, bf16[1024,1408]{1,0:T(8,128)(2,1)}, u32[]{:S(2)}) copy-start(bf16[1024,1408]{1,0:T(8,128)(2,1)} %param.24) | copy-start | bytes 8650756
  7.2 64.6 %all-reduce.10.cloned.1.call-start = ((), (), s32[]{:S(2)}) async-start(), calls=%async_computation.13 | async-start | bytes 720896 | tf_op jit(solution)/shard_map/psum | solution.py:46
  7.2 18.2 %copy-start.3 = (bf16[1024,1408]{1,0:T(8,128)(2,1)S(1)}, bf16[1024,1408]{1,0:T(8,128)(2,1)}, u32[]{:S(2)}) copy-start(bf16[1024,1408]{1,0:T(8,128)(2,1)} %param.23) | copy-start | bytes 8650756
  26.7 48.6 %copy-start.12 = (bf16[128]{0:T(256)(128)(2,1)S(1)}, bf16[128]{0:T(256)(128)(2,1)}, u32[]{:S(2)}) copy-start(bf16[128]{0:T(256)(128)(2,1)} %param.34) | copy-start | bytes 772
  26.7 48.6 %copy-start.7 = (bf16[1024]{0:T(1024)(128)(2,1)S(1)}, bf16[1024]{0:T(1024)(128)(2,1)}, u32[]{:S(2)}) copy-start(bf16[1024]{0:T(1024)(128)(2,1)} %param.26) | copy-start | bytes 6148
  26.7 48.6 %copy-start.14 = (u32[32]{0:T(128)S(1)}, u32[32]{0:T(128)}, u32[]{:S(2)}) copy-start(u32[32]{0:T(128)} %constant.47) | copy-start | bytes 388
  26.7 49.9 %copy-start.13 = (f32[4]{0:T(128)S(1)}, f32[4]{0:T(128)}, u32[]{:S(2)}) copy-start(f32[4]{0:T(128)} %param.32) | copy-start | bytes 52
  26.7 79.3 %copy-start.6 = (bf16[8,1024]{1,0:T(8,128)(2,1)S(1)}, bf16[8,1024]{1,0:T(8,128)(2,1)}, u32[]{:S(2)}) copy-start(bf16[8,1024]{1,0:T(8,128)(2,1)} %param.20) | copy-start | bytes 49156
  26.7 103.9 %copy-start.10 = (bf16[1024,32]{0,1:T(8,128)(2,1)S(1)}, bf16[1024,32]{0,1:T(8,128)(2,1)}, u32[]{:S(2)}) copy-start(bf16[1024,32]{0,1:T(8,128)(2,1)} %param.30) | copy-start | bytes 196612
  26.7 104.0 %copy-start.11 = (bf16[1024,32]{0,1:T(8,128)(2,1)S(1)}, bf16[1024,32]{0,1:T(8,128)(2,1)}, u32[]{:S(2)}) copy-start(bf16[1024,32]{0,1:T(8,128)(2,1)} %param.31) | copy-start | bytes 196612
  26.7 79.2 %reduce-scatter.7.cloned.1.call-start = ((), (), s32[]{:S(2)}) async-start(), calls=%async_computation.6 | async-start | bytes 147456 | tf_op jit(solution)/shard_map/reduce_scatter | solution.py:53
  75.2 76.9 %copy-start.9 = (f32[4]{0:T(128)S(1)}, f32[4]{0:T(128)}, u32[]{:S(2)}) copy-start(f32[4]{0:T(128)} %param.33) | copy-start | bytes 52
  75.2 78.6 %reduce-scatter.11.cloned.1.call-start = ((), (), s32[]{:S(2)}) async-start(), calls=%async_computation.8 | async-start | bytes 81920 | tf_op jit(solution)/shard_map/reduce_scatter | solution.py:98
  133.1 47.3 %reduce-scatter.9.cloned.1.call-start = ((), (), s32[]{:S(2)}) async-start(), calls=%async_computation.7 | async-start | bytes 81920 | tf_op jit(solution)/shard_map/reduce_scatter | solution.py:92
  149.8 57.3 %reduce-scatter.13.cloned.1.call-start = ((), (), s32[]{:S(2)}) async-start(), calls=%async_computation.9 | async-start | bytes 81920 | tf_op jit(solution)/shard_map/reduce_scatter | solution.py:104
  152.0 109.3 %reduce-scatter.15.cloned.1.call-start = ((), (), s32[]{:S(2)}) async-start(), calls=%async_computation.10 | async-start | bytes 147456 | tf_op jit(solution)/shard_map/reduce_scatter | solution.py:53
  208.4 5.6 %copy-start.1 = (f32[16,4,128,128]{3,2,1,0:T(8,128)S(1)}, f32[16,4,128,128]{3,2,1,0:T(8,128)}, u32[]{:S(2)}) copy-start(f32[16,4,128,128]{3,2,1,0:T(8,128)} %param.21) | copy-start | bytes 12582916
  215.5 2.0 copy-start.2
  215.5 14.1 %copy-start.5 = (bf16[512,1024]{1,0:T(8,128)(2,1)S(1)}, bf16[512,1024]{1,0:T(8,128)(2,1)}, u32[]{:S(2)}) copy-start(bf16[512,1024]{1,0:T(8,128)(2,1)} %param.35) | copy-start | bytes 3145732
  217.5 13.1 %copy-start.8 = (bf16[1024]{0:T(1024)(128)(2,1)S(1)}, bf16[1024]{0:T(1024)(128)(2,1)}, u32[]{:S(2)}) copy-start(bf16[1024]{0:T(1024)(128)(2,1)} %param.36) | copy-start | bytes 6148
  230.5 92.4 %all-reduce.8.cloned.1.call-start = ((), (), s32[]{:S(2)}) async-start(), calls=%async_computation.12 | async-start | bytes 720896 | tf_op jit(solution)/shard_map/psum | solution.py:46
  261.3 18.0 %copy-start.4 = (bf16[1024,1408]{1,0:T(8,128)(2,1)S(1)}, bf16[1024,1408]{1,0:T(8,128)(2,1)}, u32[]{:S(2)}) copy-start(bf16[1024,1408]{1,0:T(8,128)(2,1)} %param.37) | copy-start | bytes 8650756
  280.6 76.4 %reduce-scatter.17.cloned.1.call-start = ((), (), s32[]{:S(2)}) async-start(), calls=%async_computation.11 | async-start | bytes 147456 | tf_op jit(solution)/shard_map/reduce_scatter | solution.py:53
Sparse Core Ops, SparseCore 0:
  26.9 44.9 all-reduce.9
  75.3 30.5 reduce-scatter.6
  133.2 20.5 reduce-scatter.10
  156.4 23.9 reduce-scatter.8
  183.0 24.0 reduce-scatter.12
  230.7 30.5 reduce-scatter.14
  280.7 42.1 all-reduce.7
  326.4 30.5 reduce-scatter.16
where the time goes:
time: 366 us; the launch traced here: 365 us
  waiting for transfers between devices  213 us (58%)
  blocking collectives  96.6 us (26%)
  matrix products  30.4 us (8%)
  between operations  15.1 us (4%)
  other arithmetic  7.24 us (2%)
    reduce_scatter x3, waiting for transfers between devices, settle(): lax.psum_scatter(partial_value.astype(jnp.bfloat16), 'tp', scatter_dimens...  90.8 us
    psum x2, waiting for transfers between devices, half_block(): lax.psum(up_part.astype(jnp.bfloat16), 'kv').astype(jnp.float32)  66.9 us
    all_gather x3, blocking collectives, spread(): return lax.all_gather(own_rows, 'tp', axis=0, tiled=True)  44.1 us
    psum x3, blocking collectives, inverse_rms(): squares = lax.psum(jnp.sum(values * values, axis=1), 'kv')  29.9 us
    reduce_scatter x1, waiting for transfers between devices, on_device(): lax.psum_scatter(jnp.dot(scaled, w_value, preferred_element_type=jnp.floa...  26.7 us
    reduce_scatter x1, waiting for transfers between devices, on_device(): lax.psum_scatter(jnp.dot(scaled, w_query, preferred_element_type=jnp.floa...  26.6 us
    unnamed x1, blocking collectives  14.4 us
    all_gather x1, blocking collectives, on_device(): lax.all_gather(normed, 'kv', axis=0, tiled=True)  8.19 us
  transfers between devices with their start and end apart: 8, of which 8 were waited for; matrix products, arithmetic and copies ran while one was open for 1% of the time, Pallas kernels for 0%

commit v1 on v0

v1 whole, which is shorter than its diff:
```python
import functools
from types import SimpleNamespace
from typing import Any, NamedTuple

import jax
import jax.numpy as jnp
from jax import lax
from jax.experimental import pallas as pl
from jax.experimental.pallas import tpu as pltpu
from jax.sharding import PartitionSpec as P

EPS = 1e-06
F32 = jnp.float32
BF16 = jnp.bfloat16
LANES = 128
OUT_STEP = 1024
MESH = pl.DeviceIdType.MESH


class Given(NamedTuple):
    tokens: Any
    state: Any
    gain_pre: Any
    w_gate_pre: Any
    w_up_pre: Any
    w_down_pre: Any
    gain_mix: Any
    w_query: Any
    w_key: Any
    w_value: Any
    w_decay: Any
    w_blend: Any
    decay_base: Any
    decay_shift: Any
    head_gain: Any
    w_out: Any
    gain_post: Any
    w_gate_post: Any
    w_up_post: Any
    w_down_post: Any


class Loads(NamedTuple):
    tokens: Any
    gain_pre: Any
    gain_mix: Any
    gain_post: Any
    head_gain: Any
    decay_base: Any
    decay_shift: Any
    w_gate_pre: Any
    w_up_pre: Any
    w_down_pre: Any
    w_decay: Any
    w_blend: Any
    w_key: Any
    w_query: Any
    w_value: Any
    state: Any
    w_out: Any
    w_gate_post: Any
    w_up_post: Any
    w_down_post: Any


NAMES = Given._fields
LOADS = Loads._fields
SMALL = LOADS[1:7]


def cuts(extent, step):
    return [(start, min(start + step, extent)) for start in range(0, extent, step)]


def layer_kernel(n_kv, n_tp, scratch_names, *refs):
    ins = Given(*refs[: len(NAMES)])
    result_ref, new_state_ref = refs[len(NAMES) : len(NAMES) + 2]
    s = SimpleNamespace(**dict(zip(scratch_names, refs[len(NAMES) + 2 :])))

    loads = Loads(
        *[
            pltpu.make_async_copy(getattr(ins, name), getattr(s, name), s.load_sem.at[i])
            for i, name in enumerate(LOADS)
        ]
    )
    first_loads = len(SMALL) + 3
    for copy in loads[:first_loads]:
        copy.start()

    kv = lax.axis_index("kv")
    tp = lax.axis_index("tp")
    own_count, chans = s.tokens.shape
    rows = own_count * n_tp
    seqs = rows // n_kv
    d_model = chans * n_kv
    wide = cuts(chans, OUT_STEP)

    def kv_peer(k):
        return lax.rem(kv + k, n_kv)

    def tp_peer(k):
        return lax.rem(tp + k, n_tp)

    barrier = pltpu.get_barrier_semaphore()
    for k in range(1, n_kv):
        pl.semaphore_signal(barrier, inc=1, device_id={"kv": kv_peer(k)}, device_id_type=MESH)
    for k in range(1, n_tp):
        pl.semaphore_signal(barrier, inc=1, device_id={"tp": tp_peer(k)}, device_id_type=MESH)
    pl.semaphore_wait(barrier, n_kv + n_tp - 2)

    sent = []

    def send(src, dst, phase, index, axis, peer):
        copy = pltpu.make_async_remote_copy(
            src_ref=src,
            dst_ref=dst,
            send_sem=getattr(s, phase + "_send").at[index],
            recv_sem=getattr(s, phase + "_recv").at[index],
            device_id={axis: peer},
            device_id_type=MESH,
        )
        copy.start()
        sent.append(copy)
        return copy

    def gather_rows(stream, phase, chunk, lo, hi):
        mine = stream.at[tp, :, lo:hi]
        return [
            send(mine, mine, phase, chunk * n_tp + k, "tp", tp_peer(k)) for k in range(1, n_tp)
        ]

    def gained_rows(stream, gain):
        values = stream[...].astype(F32).reshape(rows, chans)
        scaled = (values * s_small(gain)).astype(BF16)
        squares = values * values
        part = squares[:, :LANES]
        for lo in range(LANES, chans, LANES):
            part = part + squares[:, lo : lo + LANES]
        return scaled, part.reshape(n_kv, seqs, LANES)

    def s_small(name):
        return getattr(s, name)[...].astype(F32).reshape(1, -1)

    def spread_squares(part, phase):
        own, got = getattr(s, phase + "_own"), getattr(s, phase + "_got")
        own[...] = part
        return [
            send(own.at[kv_peer(k)], got.at[k], phase, k, "kv", kv_peer(k)) for k in range(1, n_kv)
        ]

    def inverse(copies, phase):
        for copy in copies:
            copy.wait_recv()
        total = getattr(s, phase + "_own")[kv]
        for k in range(1, n_kv):
            total = total + getattr(s, phase + "_got")[k]
        return lax.rsqrt(jnp.sum(total, axis=1, keepdims=True) / d_model + EPS)

    def settle_and_spread(left, weight_name, phase, base, share, stream_next, meanwhile=None):
        weight = getattr(s, weight_name)
        own, got = getattr(s, phase + "_own"), getattr(s, phase + "_got")
        moves = []
        for chunk, (lo, hi) in enumerate(wide):
            product = jnp.dot(left, weight[:, lo:hi], preferred_element_type=F32)
            own[:, :, lo:hi] = product.reshape(n_tp, own_count, hi - lo).astype(BF16)
            moves.append(
                [
                    send(
                        own.at[tp_peer(k), :, lo:hi],
                        got.at[k, :, lo:hi],
                        phase,
                        chunk * n_tp + k,
                        "tp",
                        tp_peer(k),
                    )
                    for k in range(1, n_tp)
                ]
            )
        if meanwhile is not None:
            meanwhile()
        spreads = []
        for chunk, (lo, hi) in enumerate(wide):
            for copy in moves[chunk]:
                copy.wait_recv()
            total = own[tp, :, lo:hi].astype(F32)
            for k in range(1, n_tp):
                total = total + got[k, :, lo:hi].astype(F32)
            fresh = (base(lo, hi) + share * total).astype(BF16)
            if stream_next is None:
                result_ref[:, lo:hi] = fresh
            else:
                getattr(s, stream_next)[tp, :, lo:hi] = fresh
                spreads += gather_rows(getattr(s, stream_next), stream_next, chunk, lo, hi)
        return spreads

    def half_block(stream_name, spreads, tag):
        for copy in spreads:
            copy.wait_recv()
        scaled, squares = gained_rows(getattr(s, stream_name), "gain_" + tag)
        square_moves = spread_squares(squares, "sq_" + tag)
        gate, up = getattr(s, "w_gate_" + tag), getattr(s, "w_up_" + tag)
        own, got, hidden = getattr(s, "gu_" + tag + "_own"), getattr(s, "gu_" + tag + "_got"), getattr(s, "hid_" + tag)
        columns = cuts(gate.shape[1], 512)
        getattr(loads, "w_gate_" + tag).wait()
        getattr(loads, "w_up_" + tag).wait()
        if tag == "pre":
            for copy in loads[first_loads:]:
                copy.start()
        moves = []
        for chunk, (lo, hi) in enumerate(columns):
            for side, weight in enumerate((gate, up)):
                product = jnp.dot(scaled, weight[:, lo:hi], preferred_element_type=F32)
                own[:, side, :, lo:hi] = product.astype(BF16).reshape(n_kv, seqs, hi - lo)
            moves.append(
                [
                    send(
                        own.at[kv_peer(k), :, :, lo:hi],
                        got.at[k, :, :, lo:hi],
                        "gu_" + tag,
                        chunk * n_kv + k,
                        "kv",
                        kv_peer(k),
                    )
                    for k in range(1, n_kv)
                ]
            )
        factor = inverse(square_moves, "sq_" + tag)
        spreads = []
        for chunk, (lo, hi) in enumerate(columns):
            for copy in moves[chunk]:
                copy.wait_recv()
            total = own[kv, :, :, lo:hi].astype(F32)
            for k in range(1, n_kv):
                total = total + got[k, :, :, lo:hi].astype(F32)
            gated = factor * total[0]
            value = gated * jax.nn.sigmoid(gated) * (factor * total[1])
            hidden[kv, :, lo:hi] = value.astype(BF16)
            mine = hidden.at[kv, :, lo:hi]
            spreads += [
                send(mine, mine, "hid_" + tag, chunk * n_kv + k, "kv", kv_peer(k))
                for k in range(1, n_kv)
            ]
        for copy in spreads:
            copy.wait_recv()
        getattr(loads, "w_down_" + tag).wait()
        return hidden[...].reshape(rows, gate.shape[1])

    loads.tokens.wait()
    s.stream_a[tp] = s.tokens[...]
    spreads = gather_rows(s.stream_a, "stream_a", 0, 0, chans)
    for copy in loads[1 : 1 + len(SMALL)]:
        copy.wait()
    hidden = half_block("stream_a", spreads, "pre")
    spreads = settle_and_spread(
        hidden,
        "w_down_pre",
        "rs_pre",
        lambda lo, hi: s.tokens[:, lo:hi].astype(F32),
        0.5,
        "stream_b",
    )

    for copy in spreads:
        copy.wait_recv()
    scaled, squares = gained_rows(s.stream_b, "gain_mix")
    square_moves = spread_squares(squares, "sq_mix")
    heads_all = s.w_decay.shape[0]
    loads.w_decay.wait()
    loads.w_blend.wait()
    for side, weight in enumerate((s.w_decay, s.w_blend)):
        product = lax.dot_general(
            scaled, weight[...], (((1,), (1,)), ((), ())), preferred_element_type=F32
        )
        s.db_own[:, side] = product.astype(BF16).reshape(n_kv, seqs, heads_all)
    db_moves = [
        send(s.db_own.at[kv_peer(k)], s.db_got.at[k], "db", k, "kv", kv_peer(k))
        for k in range(1, n_kv)
    ]
    width = s.w_key.shape[1]
    qkv_moves = []
    for side, name in enumerate(("w_key", "w_query", "w_value")):
        getattr(loads, name).wait()
        product = jnp.dot(scaled, getattr(s, name)[...], preferred_element_type=F32)
        s.qkv_own[:, side] = product.astype(BF16).reshape(n_kv, seqs, width)
        qkv_moves.append(
            [
                send(
                    s.qkv_own.at[kv_peer(k), side],
                    s.qkv_got.at[k, side],
                    "qkv",
                    side * n_kv + k,
                    "kv",
                    kv_peer(k),
                )
                for k in range(1, n_kv)
            ]
        )
    factor = inverse(square_moves, "sq_mix")
    for copy in db_moves:
        copy.wait_recv()
    gates = s.db_own[kv].astype(F32)
    for k in range(1, n_kv):
        gates = gates + s.db_got[k].astype(F32)
    state = s.state
    heads = state.shape[1]
    head_dim = state.shape[3]
    lane = lax.broadcasted_iota(jnp.int32, (seqs, heads_all), 1)
    for h in range(heads):
        chosen = lane == tp * heads + h
        decay_in = factor * jnp.sum(jnp.where(chosen, gates[0], 0.0), axis=1, keepdims=True)
        blend_in = factor * jnp.sum(jnp.where(chosen, gates[1], 0.0), axis=1, keepdims=True)
        base = jnp.broadcast_to(s.decay_base[:, h : h + 1], (seqs, head_dim))
        shifted = decay_in + jnp.broadcast_to(s.decay_shift[:, h : h + 1], (seqs, head_dim))
        soft = jnp.maximum(shifted, 0.0) + jnp.log1p(jnp.exp(-jnp.abs(shifted)))
        s.rate[h] = jnp.exp(-jnp.exp(base) * soft)
        s.beta[h] = jnp.broadcast_to(jax.nn.sigmoid(blend_in), (seqs, head_dim))

    def summed(side):
        for copy in qkv_moves[side]:
            copy.wait_recv()
        total = s.qkv_own[kv, side].astype(F32)
        for k in range(1, n_kv):
            total = total + s.qkv_got[k, side].astype(F32)
        return factor * total

    def unit(values):
        return values * lax.rsqrt(jnp.sum(values * values, axis=-1, keepdims=True) + EPS)

    keys = summed(0)
    queries = summed(1)
    stacked = [unit(keys[:, h * head_dim : (h + 1) * head_dim]) for h in range(heads)]
    stacked += [
        unit(queries[:, h * head_dim : (h + 1) * head_dim]) * head_dim ** (-0.5)
        for h in range(heads)
    ]
    for h in range(heads):
        s.key[h] = stacked[h]
        s.query[h] = stacked[heads + h]
    values_new = summed(2)
    loads.state.wait()

    place = lax.broadcasted_iota(jnp.int32, (8, head_dim), 0)

    def recall(b, carry):
        at = pl.ds(b, 1)
        for h in range(heads):
            pair = jnp.where(
                place == 0, s.key[h, at, :], jnp.where(place == 1, s.query[h, at, :], 0.0)
            )
            answer = jnp.dot(
                pair, state[b, h], preferred_element_type=F32, precision=lax.Precision.HIGHEST
            )
            s.recalled[h, at, :] = answer[0:1]
            s.past[h, at, :] = answer[1:2]
        return carry

    lax.fori_loop(0, seqs, recall, 0, unroll=4)
    for h in range(heads):
        value = values_new[:, h * head_dim : (h + 1) * head_dim]
        correction = s.beta[h] * (value - s.rate[h] * s.recalled[h])
        s.correction[h] = correction
        overlap = jnp.sum(stacked[h] * stacked[heads + h], axis=1, keepdims=True)
        read = s.rate[h] * s.past[h] + overlap * correction
        normed = read * lax.rsqrt(jnp.mean(read * read, axis=1, keepdims=True) + EPS)
        normed = normed * s_small("head_gain")
        s.normed[kv, :, h * head_dim : (h + 1) * head_dim] = normed.astype(BF16)
    store = pltpu.make_async_copy(state, new_state_ref, s.store_sem.at[0])

    def update_state():
        turned_keys = stacked[:heads]
        left_over = LANES - heads * seqs
        if left_over:
            turned_keys = turned_keys + [jnp.zeros((left_over, head_dim), F32)]
        s.columns[...] = jnp.concatenate(turned_keys, axis=0).T

        def one_sequence(b, carry):
            turned = pltpu.roll(s.columns[...], lax.rem(LANES - b, LANES), 1)
            at = pl.ds(b, 1)
            for h in range(heads):
                key = turned[:, h * seqs : h * seqs + 1]
                state[b, h] = s.rate[h, at, :] * state[b, h] + key * s.correction[h, at, :]
            return carry

        lax.fori_loop(0, seqs, one_sequence, 0)
        store.start()

    mine = s.normed.at[kv]
    spreads = [send(mine, mine, "normed", k, "kv", kv_peer(k)) for k in range(1, n_kv)]
    for copy in spreads:
        copy.wait_recv()
    loads.w_out.wait()
    spreads = settle_and_spread(
        s.normed[...].reshape(rows, width),
        "w_out",
        "rs_mix",
        lambda lo, hi: s.stream_b[tp, :, lo:hi].astype(F32),
        1.0,
        "stream_c",
        update_state,
    )

    hidden = half_block("stream_c", spreads, "post")
    settle_and_spread(
        hidden,
        "w_down_post",
        "rs_post",
        lambda lo, hi: s.stream_c[tp, :, lo:hi].astype(F32),
        0.5,
        None,
    )
    for copy in sent:
        copy.wait_send()
    store.wait()


def output_kernel(result_in, state_in, result_out, state_out, rows, held, in_sem, out_sem):
    pieces = [(result_in, rows, result_out)]
    step = 2 if held.shape[0] % 2 == 0 else 1
    for b in range(0, held.shape[0], step):
        at = pl.ds(b, step)
        pieces.append((state_in.at[at], held.at[at], state_out.at[at]))
    taken = [
        pltpu.make_async_copy(source, middle, in_sem.at[i])
        for i, (source, middle, target) in enumerate(pieces)
    ]
    for copy in taken:
        copy.start()
    given_out = []
    for i, (source, middle, target) in enumerate(pieces):
        taken[i].wait()
        copy = pltpu.make_async_copy(middle, target, out_sem.at[i])
        copy.start()
        given_out.append(copy)
    for copy in given_out:
        copy.wait()


def on_device(n_kv, n_tp, *args):
    given = SimpleNamespace(**dict(zip(NAMES, args)))
    own_count, chans = given.tokens.shape
    rows = own_count * n_tp
    seqs = rows // n_kv
    ff = given.w_gate_pre.shape[1]
    width = given.w_query.shape[1]
    heads, head_dim = given.state.shape[1], given.state.shape[3]
    given.w_decay, given.w_blend = given.w_decay.T, given.w_blend.T
    given.decay_base = given.decay_base.reshape(1, -1)
    given.decay_shift = given.decay_shift.reshape(1, -1)
    heads_all = given.w_decay.shape[0]
    out_steps = len(cuts(chans, OUT_STEP))
    ff_steps = len(cuts(ff, 512))
    scratch = {name: pltpu.VMEM(getattr(given, name).shape, getattr(given, name).dtype) for name in LOADS}
    scratch["load_sem"] = pltpu.SemaphoreType.DMA((len(LOADS),))
    scratch["store_sem"] = pltpu.SemaphoreType.DMA((1,))

    def semaphores(phase, count):
        scratch[phase + "_send"] = pltpu.SemaphoreType.DMA((count,))
        scratch[phase + "_recv"] = pltpu.SemaphoreType.DMA((count,))

    for name in ("stream_a", "stream_b", "stream_c"):
        scratch[name] = pltpu.VMEM((n_tp, own_count, chans), BF16)
        semaphores(name, n_tp * out_steps)
    for tag in ("pre", "post", "mix"):
        scratch["sq_" + tag + "_own"] = pltpu.VMEM((n_kv, seqs, LANES), F32)
        scratch["sq_" + tag + "_got"] = pltpu.VMEM((n_kv, seqs, LANES), F32)
        semaphores("sq_" + tag, n_kv)
        scratch["rs_" + tag + "_own"] = pltpu.VMEM((n_tp, own_count, chans), BF16)
        scratch["rs_" + tag + "_got"] = pltpu.VMEM((n_tp, own_count, chans), BF16)
        semaphores("rs_" + tag, n_tp * out_steps)
    for tag in ("pre", "post"):
        scratch["gu_" + tag + "_own"] = pltpu.VMEM((n_kv, 2, seqs, ff), BF16)
        scratch["gu_" + tag + "_got"] = pltpu.VMEM((n_kv, 2, seqs, ff), BF16)
        semaphores("gu_" + tag, n_kv * ff_steps)
        scratch["hid_" + tag] = pltpu.VMEM((n_kv, seqs, ff), BF16)
        semaphores("hid_" + tag, n_kv * ff_steps)
    for name in ("db_own", "db_got"):
        scratch[name] = pltpu.VMEM((n_kv, 2, seqs, heads_all), BF16)
    semaphores("db", n_kv)
    for name in ("qkv_own", "qkv_got"):
        scratch[name] = pltpu.VMEM((n_kv, 3, seqs, width), BF16)
    semaphores("qkv", 3 * n_kv)
    for name in ("rate", "beta", "key", "query", "recalled", "past", "correction"):
        scratch[name] = pltpu.VMEM((heads, seqs, head_dim), F32)
    scratch["columns"] = pltpu.VMEM((head_dim, LANES), F32)
    scratch["normed"] = pltpu.VMEM((n_kv, seqs, width), BF16)
    semaphores("normed", n_kv)

    anywhere = pl.BlockSpec(memory_space=pl.ANY)
    in_vmem = pl.BlockSpec(memory_space=pltpu.VMEM)
    out_shape = (
        jax.ShapeDtypeStruct(given.tokens.shape, BF16),
        jax.ShapeDtypeStruct(given.state.shape, F32),
    )
    result, new_state = pl.pallas_call(
        functools.partial(layer_kernel, n_kv, n_tp, tuple(scratch)),
        out_shape=out_shape,
        in_specs=[anywhere] * len(NAMES),
        out_specs=(in_vmem, anywhere),
        scratch_shapes=list(scratch.values()),
        compiler_params=pltpu.CompilerParams(collective_id=0, has_side_effects=True),
    )(*[getattr(given, name) for name in NAMES])
    return pl.pallas_call(
        output_kernel,
        out_shape=out_shape,
        in_specs=[anywhere, anywhere],
        out_specs=(anywhere, anywhere),
        scratch_shapes=[
            pltpu.VMEM(given.tokens.shape, BF16),
            pltpu.VMEM(given.state.shape, F32),
            pltpu.SemaphoreType.DMA((seqs + 1,)),
            pltpu.SemaphoreType.DMA((seqs + 1,)),
        ],
    )(result, new_state)


def solution(mesh):
    return jax.shard_map(
        functools.partial(on_device, mesh.shape["kv"], mesh.shape["tp"]),
        mesh=mesh,
        in_specs=(
            P("tp", "kv"),
            P("kv", "tp", None, None),
            P("kv"),
            P("kv", "tp"),
            P("kv", "tp"),
            P("tp", "kv"),
            P("kv"),
            P("kv", "tp"),
            P("kv", "tp"),
            P("kv", "tp"),
            P("kv", None),
            P("kv", None),
            P("tp"),
            P("tp"),
            P(),
            P("tp", "kv"),
            P("kv"),
            P("kv", "tp"),
            P("kv", "tp"),
            P("tp", "kv"),
        ),
        out_specs=(P("tp", "kv"), P("kv", "tp", None, None)),
        check_vma=False,
    )
```

time: 366 us -> 74.1 us (0.20)
  waiting for transfers between devices: 213 us -> 0 us
  blocking collectives: 96.6 us -> 0 us
  Pallas kernels: 0 us -> 73.1 us
  matrix products: 30.4 us -> 0 us
  between operations: 15.1 us -> 0.65 us
  other arithmetic: 7.24 us -> 0 us
    reduce_scatter x6 -> x0, waiting for transfers between devices: 146 us -> none  [the longest x3 90.8 us: settle(): lax.psum_scatter(partial_value.astype(jnp.bfloat16), 'tp', scatter_dimens...]
    pallas_call x0 -> x2, Pallas kernels: none -> 73.1 us  [the longest x1 69.3 us: on_device(): pl.pallas_call(functools.partial(layer_kernel, n_kv, n_tp, tuple(scratch)...]
    psum x2 -> x0, waiting for transfers between devices: 66.9 us -> none  [half_block(): lax.psum(up_part.astype(jnp.bfloat16), 'kv').astype(jnp.float32)]
    all_gather x4 -> x0, blocking collectives: 52.3 us -> none  [the longest x3 44.1 us: spread(): return lax.all_gather(own_rows, 'tp', axis=0, tiled=True)]
    dot_general x14 -> x0, matrix products: 30.4 us -> none  [the longest x2 6.7 us: half_block(): return jnp.dot(hidden, w_down, preferred_element_type=jnp.float32)]
    psum x3 -> x0, blocking collectives: 29.9 us -> none  [inverse_rms(): squares = lax.psum(jnp.sum(values * values, axis=1), 'kv')]
    unnamed x1 -> x0, blocking collectives: 14.4 us -> none
    convert_element_type x8 -> x0, other arithmetic: 3.86 us -> none  [the longest x3 2.93 us: residual_add(): return (stream.astype(jnp.float32) + weight * branch).astype(jnp.bfloat16)]
  transfers between devices with their start and end apart: 8 -> 0, of which waited for: 8 -> 0; matrix products, arithmetic and copies ran while one was open for 1% -> 0% of each run, Pallas kernels for 0% -> 0%
where the time goes in v1:
time: 74.1 us; the launch traced here: 73.8 us
  Pallas kernels  73.1 us (99%)
    pallas_call x1, Pallas kernels, on_device(): pl.pallas_call(functools.partial(layer_kernel, n_kv, n_tp, tuple(scratch)...  69.3 us
    pallas_call x1, Pallas kernels, on_device(): pl.pallas_call(output_kernel, out_shape=out_shape, in_specs=[anywhere, an...  3.78 us

profile of v1, /device:TPU:0, one launch (start us, length us, event | category | flops | bytes accessed | tf_op | source)
XLA Modules:
  0.0 73.8 jit_solution(16095485635727451671)
XLA Ops:
  0.6 69.3 %shard_map.203 = (bf16[8,1024]{1,0:T(8,128)(2,1)}, f32[16,4,128,128]{3,2,1,0:T(8,128)}) custom-call(bf16[8,1024]{1,0:T(8,128)(2,1)} %refs_0_.1, f32[16,4,128,128]{3,2,1,0:T(8,128)} %refs_1_.1, bf16[1024]{0:T(1024)(128)(2,1)} %refs_2_.1, bf16[1024,1408]{1,0:T(8,128)(2,1)} %refs_3_.1, bf16[1024,1408]{1,0:T(8,128)(2,1)} %refs_4_.1, bf16[1408,1024]{1,0:T(8,128)(2,1)} %refs_5_.1, ...), custom_call_target="tpu_custom_call" | custom-call | tf_op jit(solution)/shard_map/pallas_call | solution.py:494
  70.0 3.8 %shard_map.204 = (bf16[8,1024]{1,0:T(8,128)(2,1)}, f32[16,4,128,128]{3,2,1,0:T(8,128)}) custom-call(bf16[8,1024]{1,0:T(8,128)(2,1)} %get-tuple-element.4.result_in, f32[16,4,128,128]{3,2,1,0:T(8,128)} %get-tuple-element.5.state_in), custom_call_target="tpu_custom_call" | custom-call | tf_op jit(solution)/shard_map/pallas_call | solution.py:502
